TPU v7x, 32 devices: a whole 2x2x4 slice. The times are simulated.
32 devices in a mesh: ep: 8 (over z, core), tp: 4 (over y, x).
Axes of the slice: x: 2, y: 2, z: 4, core: 2. Of those that a mesh axis runs over, the one named last changes fastest.
Arguments:
- tokens: bfloat16 [1024, 2048], P('ep'), may hold values from -6 to 6
- cotangent: bfloat16 [1024, 2048], P('ep'), may hold values from -6 to 6
- expert_ids: int32 [1024, 2], P('ep'), may hold values from 0 to 7, all different within a row; in each aligned block of 128 rows (0 to 127, 128 to 255, ...) at most 64 rows name the same one
- route_weight: bfloat16 [1024, 2], P('ep'), may hold values from 0.19921875 to 1
- gate_weight: bfloat16 [8, 1024, 2048], P('ep', 'tp'), may hold values from -0.125 to 0.125
- up_weight: bfloat16 [8, 1024, 2048], P('ep', 'tp'), may hold values from -0.125 to 0.125
- down_weight: bfloat16 [8, 1024, 2048], P('ep', 'tp'), may hold values from -0.1875 to 0.1875
Outputs:
- tokens_grad: bfloat16 [1024, 2048], P('ep', 'tp')
- route_weight_grad: float32 [1024, 2], P('ep')
- gate_weight_grad: float32 [8, 1024, 2048], P('ep', 'tp')
- up_weight_grad: float32 [8, 1024, 2048], P('ep', 'tp')
- down_weight_grad: float32 [8, 1024, 2048], P('ep', 'tp')
Inputs may be any that keep to these rules, and one draw needn't show every extreme that they name: `expert_ids`: within each aligned block of 128 rows every expert is named at most 64 times; the two experts of a row differ.
All inputs are finite; a program needn't handle non-finite values.
Results may differ from a plain program's by a relative error of at most 0.0058.
Values may be sent and summed in bfloat16 or wider, within the bound.
A program may use at most 64 MiB of HBM per device.

v0:
```python
import jax
import jax.numpy as jnp
from jax import lax
from jax.sharding import PartitionSpec as P


def per_device(tokens, cotangent, expert_ids, route_weight, gate_weight, up_weight, down_weight):
    tok_rows, model_width = tokens.shape
    top_count = expert_ids.shape[1]
    local_experts = gate_weight.shape[0]
    ep_size = lax.axis_size("ep")
    tp_size = lax.axis_size("tp")
    expert_count = local_experts * ep_size
    capacity = 2 * tok_rows * top_count // expert_count
    column_span = model_width // tp_size
    flat_ids = expert_ids.reshape(-1)
    routed = flat_ids.shape[0]
    member = (flat_ids[:, None] == jnp.arange(expert_count, dtype=jnp.int32)[None, :]).astype(
        jnp.int32
    )
    rank_slot = jnp.sum((jnp.cumsum(member, axis=0) - 1) * member, axis=1)
    slot_index = flat_ids * capacity + rank_slot
    buffer_rows = expert_count * capacity
    source_pair = (
        jnp.full((buffer_rows,), routed, jnp.int32)
        .at[slot_index]
        .set(jnp.arange(routed, dtype=jnp.int32))
    )
    filled = source_pair < routed
    safe_pair = jnp.minimum(source_pair, routed - 1)
    token_of = safe_pair // top_count
    zero_value = jnp.zeros((), tokens.dtype)
    send_weight = jnp.where(filled, route_weight.reshape(-1)[safe_pair], zero_value)
    offset = lax.axis_index("tp") * column_span
    token_cols = lax.dynamic_slice_in_dim(tokens, offset, column_span, 1)
    cotangent_cols = lax.dynamic_slice_in_dim(cotangent, offset, column_span, 1)
    part_tokens, part_cotangent, got_weight = (
        lax.all_to_all(token_cols[token_of], "ep", split_axis=0, concat_axis=0, tiled=True),
        lax.all_to_all(cotangent_cols[token_of], "ep", split_axis=0, concat_axis=0, tiled=True),
        lax.all_to_all(send_weight, "ep", split_axis=0, concat_axis=0, tiled=True),
    )
    got_tokens, got_cotangent = (
        lax.all_gather(part_tokens, "tp", axis=1, tiled=True),
        lax.all_gather(part_cotangent, "tp", axis=1, tiled=True),
    )
    block_shape = (ep_size, local_experts, capacity, model_width)
    routed_rows = got_tokens.reshape(block_shape)
    routed_cotangent = got_cotangent.reshape(block_shape)
    pair_weight = got_weight.reshape(ep_size, local_experts, capacity, 1).astype(jnp.float32)
    pre_gate = jnp.einsum(
        "secd,efd->secf", routed_rows, gate_weight, preferred_element_type=jnp.float32
    )
    pre_up = jnp.einsum(
        "secd,efd->secf", routed_rows, up_weight, preferred_element_type=jnp.float32
    )
    sigma = jax.nn.sigmoid(pre_gate)
    silu_gate = pre_gate * sigma
    hidden = silu_gate * pre_up
    back_hidden = jnp.einsum(
        "secd,efd->secf", routed_cotangent, down_weight, preferred_element_type=jnp.float32
    )
    pair_products = lax.psum(jnp.sum(hidden * back_hidden, axis=3), "tp")
    scaled = pair_weight * back_hidden
    grad_gate = (scaled * pre_up * sigma * (1.0 + pre_gate * (1.0 - sigma))).astype(jnp.bfloat16)
    grad_up = (scaled * silu_gate).astype(jnp.bfloat16)
    weighted = (pair_weight * hidden).astype(jnp.bfloat16)
    down_grad = jnp.einsum(
        "secf,secd->efd", weighted, routed_cotangent, preferred_element_type=jnp.float32
    )
    gate_grad = jnp.einsum(
        "secf,secd->efd", grad_gate, routed_rows, preferred_element_type=jnp.float32
    )
    up_grad = jnp.einsum("secf,secd->efd", grad_up, routed_rows, preferred_element_type=jnp.float32)
    full_gate, full_up = (
        lax.all_gather(grad_gate, "tp", axis=3, tiled=True),
        lax.all_gather(grad_up, "tp", axis=3, tiled=True),
    )
    gate_cols, up_cols = (
        lax.all_to_all(gate_weight, "tp", split_axis=2, concat_axis=1, tiled=True),
        lax.all_to_all(up_weight, "tp", split_axis=2, concat_axis=1, tiled=True),
    )
    pair_grad = (
        jnp.einsum("secf,efd->secd", full_gate, gate_cols, preferred_element_type=jnp.float32)
        + jnp.einsum("secf,efd->secd", full_up, up_cols, preferred_element_type=jnp.float32)
    ).astype(jnp.bfloat16)
    returned = lax.all_to_all(
        pair_grad.reshape(buffer_rows, column_span), "ep", split_axis=0, concat_axis=0, tiled=True
    )
    returned_products = lax.all_to_all(
        pair_products.reshape(buffer_rows), "ep", split_axis=0, concat_axis=0, tiled=True
    )
    per_pair = returned[slot_index].astype(jnp.float32).reshape(tok_rows, top_count, column_span)
    tokens_grad = jnp.sum(per_pair, axis=1).astype(jnp.bfloat16)
    route_grad = returned_products[slot_index].reshape(tok_rows, top_count)
    return (tokens_grad, route_grad, gate_grad, up_grad, down_grad)


def solution(mesh):
    in_specs = (
        P("ep", None),
        P("ep", None),
        P("ep", None),
        P("ep", None),
        P("ep", "tp", None),
        P("ep", "tp", None),
        P("ep", "tp", None),
    )
    out_specs = (
        P("ep", "tp"),
        P("ep", None),
        P("ep", "tp", None),
        P("ep", "tp", None),
        P("ep", "tp", None),
    )
    return jax.shard_map(
        per_device, mesh=mesh, in_specs=in_specs, out_specs=out_specs, check_vma=False
    )
```

profile of v0, /device:TPU:0, one launch (start us, length us, event | category | flops | bytes accessed | tf_op | source)
XLA Modules:
  0.0 231.4 jit_solution(7355271830630326382)
XLA Ops:
  7.2 0.8 broadcast_multiply_fusion
  8.0 0.8 copy.31
  9.3 0.6 reduce-window.6
  10.3 1.4 scatter_custom_fusion
  11.7 1.0 constant_dynamic-slice_fusion
  12.7 2.0 gather_fusion.2
  14.7 21.6 %all_to_all.85 = bf16[8,64,512]{2,1,0:T(8,128)(2,1)} all-to-all(bf16[8,64,512]{2,1,0:T(8,128)(2,1)S(1)} %bitcast.112), channel_id=1, replica_groups=mesh['ep'=8,'tp'=4] {'ep'}, dimensions={0} | all-to-all | bytes 1048576 | tf_op jit(solution)/shard_map/all_to_all | solution.py:38
  36.4 2.0 gather_fusion.1
  38.4 18.5 %all_to_all.86 = bf16[8,64,512]{2,1,0:T(8,128)(2,1)} all-to-all(bf16[8,64,512]{2,1,0:T(8,128)(2,1)S(1)} %bitcast.111), channel_id=1, replica_groups=mesh['ep'=8,'tp'=4] {'ep'}, dimensions={0} | all-to-all | bytes 1048576 | tf_op jit(solution)/shard_map/all_to_all | solution.py:39
  57.3 3.4 %gather_fusion = bf16[512]{0:T(512)(128)(2,1)S(1)} fusion(bf16[256]{0:T(256)(128)(2,1)S(1)} %reshape.155, s32[1024]{0:T(1024)S(1)} %get-tuple-element.28), kind=kCustom, calls=%fused_computation | custom fusion | bytes 4096 | tf_op jit(solution)/shard_map/gather | solution.py:33
  60.8 8.1 %all_to_all.87 = bf16[8,64,1]{1,2,0:T(2,128)(2,1)S(1)} all-to-all(bf16[8,64,1]{1,2,0:T(2,128)(2,1)S(1)} %all_to_all.77), channel_id=1, replica_groups=mesh['ep'=8,'tp'=4] {'ep'}, dimensions={0} | all-to-all | bytes 2048 | tf_op jit(solution)/shard_map/all_to_all | solution.py:40
  68.8 1.6 all-gather.7.cloned.1.call-done
  70.5 3.3 %convolution_bitcast_fusion.4 = f32[8,1,64,256]{3,2,0,1:T(8,128)} fusion(bf16[8,64,2048]{2,1,0:T(8,128)(2,1)} %bitcast.101, bf16[1,256,2048]{2,1,0:T(8,128)(2,1)S(1)} %copy-done.5), kind=kOutput, calls=%fused_computation.12 | convolution fusion | flops 536870912 | bytes 3670016 | tf_op jit(solution)/shard_map/secd,efd->secf/dot_general | solution.py:53
  73.8 0.7 convolution_bitcast_fusion.3
  74.5 32.8 %all-gather.5.cloned.1.call-done = bf16[512,2048]{1,0:T(8,128)(2,1)} async-done(((bf16[512,512]{1,0:T(8,128)(2,1)}), bf16[512,2048]{1,0:T(8,128)(2,1)}) %all-gather.5.cloned.1.call-update) | async-done | bytes 2097168 | tf_op jit(solution)/shard_map/all_gather | solution.py:44
  107.4 3.3 %multiply_reduce_fusion = (f32[8,64]{1,0:T(8,128)S(1)}, bf16[8,1,64,256]{3,2,0,1:T(8,128)(2,1)}, bf16[8,1,64,256]{3,2,0,1:T(8,128)(2,1)}) fusion(f32[8,1,64,256]{3,2,0,1:T(8,128)S(1)} %copy-done.9, f32[8,1,64,256]{3,2,0,1:T(8,128)S(1)} %convolution_bitcast_fusion.3, f32[8,64]{1,0:T(8,128)S(1)} %bitcast.117, bf16[8,64,2048]{2,1,0:T(8,128)(2,1)} %bitcast.109, ...), kind=kOutput, calls=%fused_computation.21 | convolution fusion | flops 539098624 | bytes 4722688 | tf_op jit(solution)/shard_map/secd,efd->secf/dot_general | solution.py:59
  110.6 4.6 %copy.35 = bf16[1,256,2048]{1,0,2:T(2,128)(2,1)S(1)} copy(bf16[1,256,2048]{2,1,0:T(8,128)(2,1)} %param.11) | data formatting | bytes 2097152 | tf_op args[4]
  115.3 0.5 broadcast.123
  115.8 11.6 %reduce.8 = bf16[2048,256]{1,0:T(8,128)(2,1)} reduce(bf16[2048,1,256]{2,1,0:T(2,128)(2,1)S(1)} %bitcast.105, bf16[]{:T(256)} %broadcast.123), dimensions={1}, to_apply=%bitcast.84.reduce_sub_computation | reduce | bytes 2097154
  127.3 3.5 %reshape.242 = bf16[4,2,65536]{2,1,0:T(2,128)(2,1)} reshape(bf16[2048,256]{1,0:T(8,128)(2,1)} %reduce.8) | data formatting | bytes 2097152
  130.8 4.2 %all-to-all-start.3 = ((bf16[4,2,65536]{2,1,0:T(2,128)(2,1)}), bf16[4,2,65536]{2,1,0:T(2,128)(2,1)}, u32[]{:S(2)}, u32[]{:S(2)}) async-start(bf16[4,2,65536]{2,1,0:T(2,128)(2,1)} %reshape.242), calls=%async_computation.3 | async-start | bytes 2097152 | tf_op jit(solution)/shard_map/all_to_all | solution.py:79
  135.3 0.3 all-gather.11.cloned.1.call-update
  135.6 4.6 %copy.37 = bf16[1,256,2048]{1,0,2:T(2,128)(2,1)S(1)} copy(bf16[1,256,2048]{2,1,0:T(8,128)(2,1)} %param.12) | data formatting | bytes 2097152 | tf_op args[5]
  140.3 11.6 %reduce.9 = bf16[2048,256]{1,0:T(8,128)(2,1)} reduce(bf16[2048,1,256]{2,1,0:T(2,128)(2,1)S(1)} %bitcast.106, bf16[]{:T(256)} %broadcast.123), dimensions={1}, to_apply=%bitcast.86.reduce_sub_computation | reduce | bytes 2097154
  151.8 3.5 %reshape.244 = bf16[4,2,65536]{2,1,0:T(2,128)(2,1)} reshape(bf16[2048,256]{1,0:T(8,128)(2,1)} %reduce.9) | data formatting | bytes 2097152
  155.3 4.3 %all-to-all-start.4 = ((bf16[4,2,65536]{2,1,0:T(2,128)(2,1)}), bf16[4,2,65536]{2,1,0:T(2,128)(2,1)}, u32[]{:S(2)}, u32[]{:S(2)}) async-start(bf16[4,2,65536]{2,1,0:T(2,128)(2,1)} %reshape.244), calls=%async_computation.4 | async-start | bytes 2097152 | tf_op jit(solution)/shard_map/all_to_all | solution.py:80
  159.6 2.6 %reshape.243 = bf16[2048,1,256]{2,1,0:T(2,128)(2,1)S(1)} reshape(bf16[4,2,65536]{2,1,0:T(2,128)(2,1)} %all-to-all-done.3) | data formatting | bytes 2097152
  162.2 1.1 copy.40
  163.4 2.3 copy.36
  165.6 10.7 %all-to-all-done.4 = bf16[4,2,65536]{2,1,0:T(2,128)(2,1)} async-done(((bf16[4,2,65536]{2,1,0:T(2,128)(2,1)}), bf16[4,2,65536]{2,1,0:T(2,128)(2,1)}, u32[]{:S(2)}, u32[]{:S(2)}) %all-to-all-start.4) | async-done | bytes 1048608 | tf_op jit(solution)/shard_map/all_to_all | solution.py:80
  176.4 2.6 %reshape.245 = bf16[2048,1,256]{2,1,0:T(2,128)(2,1)S(1)} reshape(bf16[4,2,65536]{2,1,0:T(2,128)(2,1)} %all-to-all-done.4) | data formatting | bytes 2097152
  179.0 1.1 copy.41
  180.1 1.6 copy.38
  181.7 9.5 %psum.7 = f32[8,64,1]{1,2,0:T(1,128)} all-reduce(f32[8,64,1]{1,2,0:T(1,128)S(1)} %bitcast.121), channel_id=1, replica_groups=mesh['ep'=8,'tp'=4] {'tp'}, use_global_device_ids=true, to_apply=%region_6.7 | all-reduce | flops 512 | bytes 4096 | tf_op jit(solution)/shard_map/psum | solution.py:62
  191.3 4.6 %all-to-all-start.6 = ((f32[8,64,1]{1,2,0:T(1,128)}), f32[8,64,1]{1,2,0:T(1,128)S(1)}, u32[]{:S(2)}, u32[]{:S(2)}) async-start(f32[8,64,1]{1,2,0:T(1,128)} %psum.7), calls=%async_computation.6 | async-start | bytes 8192 | tf_op jit(solution)/shard_map/all_to_all | solution.py:89
  195.9 2.9 %fusion.2 = f32[8,64,512]{2,1,0:T(8,128)} fusion(bf16[1024,512,1]{1,0,2:T(8,128)(2,1)S(1)} %bitcast.115, bf16[8,1,64,1024]{3,2,0,1:T(8,128)(2,1)} %all-gather.9.cloned.1.call-done), kind=kOutput, calls=%fused_computation.15 | convolution fusion | flops 536870912 | bytes 3145728 | tf_op jit(solution)/shard_map/secf,efd->secd/dot_general | solution.py:83
  198.8 3.1 %fusion = bf16[8,64,512]{2,1,0:T(8,128)(2,1)} fusion(f32[8,64,512]{2,1,0:T(8,128)} %fusion.2, bf16[1024,512,1]{1,0,2:T(8,128)(2,1)S(1)} %bitcast.116, bf16[8,1,64,1024]{3,2,0,1:T(8,128)(2,1)} %all-gather.11.cloned.1.call-done), kind=kOutput, calls=%fused_computation.10 | convolution fusion | flops 537395200 | bytes 3670016 | tf_op jit(solution)/shard_map/secf,efd->secd/dot_general | solution.py:84
  201.9 5.1 %all-to-all-start.5 = ((bf16[8,64,512]{2,1,0:T(8,128)(2,1)}), bf16[8,64,512]{2,1,0:T(8,128)(2,1)S(1)}, u32[]{:S(2)}, u32[]{:S(2)}) async-start(bf16[8,64,512]{2,1,0:T(8,128)(2,1)} %fusion), calls=%async_computation.5 | async-start | bytes 1048576 | tf_op jit(solution)/shard_map/all_to_all | solution.py:86
  207.0 3.8 %convolution_bitcast_fusion.2 = f32[1,256,2048]{2,1,0:T(8,128)} fusion(bf16[8,64,2048]{2,1,0:T(8,128)(2,1)} %bitcast.102, bf16[8,1,64,256]{3,2,0,1:T(8,128)(2,1)S(1)} %copy-done.7), kind=kOutput, calls=%fused_computation.8 | convolution fusion | flops 536870912 | bytes 4456448 | tf_op jit(solution)/shard_map/secf,secd->efd/dot_general | solution.py:70
  210.8 2.0 convolution_bitcast_fusion.1
  213.1 2.1 convolution_bitcast_fusion
  215.2 0.5 broadcast.122
  215.7 0.7 reduce.7
  216.5 1.9 gather_fusion.4
  218.6 0.6 copy.39
  219.2 3.1 %all-to-all-done.5 = bf16[8,64,512]{2,1,0:T(8,128)(2,1)S(1)} async-done(((bf16[8,64,512]{2,1,0:T(8,128)(2,1)}), bf16[8,64,512]{2,1,0:T(8,128)(2,1)S(1)}, u32[]{:S(2)}, u32[]{:S(2)}) %all-to-all-start.5) | async-done | bytes 524320 | tf_op jit(solution)/shard_map/all_to_all | solution.py:86
  222.3 1.2 gather_fusion.3
  223.6 1.3 reduce_sum.36
  (61 shorter events, 2.3 us)
Async XLA Ops:
  7.2 100.2 %copy-start = (bf16[1,256,2048]{2,1,0:T(8,128)(2,1)S(1)}, bf16[1,256,2048]{2,1,0:T(8,128)(2,1)}, u32[]{:S(2)}) copy-start(bf16[1,256,2048]{2,1,0:T(8,128)(2,1)} %param.13) | copy-start | bytes 3145732
  7.2 63.3 %all-gather.7.cloned.1.call-start = ((), (), s32[]{:S(2)}) async-start(), calls=%async_computation.8 | async-start | bytes 2621440 | tf_op jit(solution)/shard_map/all_gather | solution.py:43
  36.3 71.0 %all-gather.5.cloned.1.call-start = ((), (), s32[]{:S(2)}) async-start(), calls=%async_computation.7 | async-start | bytes 2621440 | tf_op jit(solution)/shard_map/all_gather | solution.py:44
  36.4 20.6 %copy-start.13 = (bf16[128,2]{0,1:T(2,128)(2,1)S(1)}, bf16[128,2]{0,1:T(2,128)(2,1)}, u32[]{:S(2)}) copy-start(bf16[128,2]{0,1:T(2,128)(2,1)} %param.10) | copy-start | bytes 1540
  38.4 32.1 %copy-start.5 = (bf16[1,256,2048]{2,1,0:T(8,128)(2,1)S(1)}, bf16[1,256,2048]{2,1,0:T(8,128)(2,1)}, u32[]{:S(2)}) copy-start(bf16[1,256,2048]{2,1,0:T(8,128)(2,1)} %param.12) | copy-start | bytes 3145732
  56.9 138.9 %all-gather.9.cloned.1.call-start = ((), (), s32[]{:S(2)}) async-start(), calls=%async_computation.9 | async-start | bytes 1310720 | tf_op jit(solution)/shard_map/all_gather | solution.py:75
  60.7 13.1 %copy-start.4 = (bf16[1,256,2048]{2,1,0:T(8,128)(2,1)S(1)}, bf16[1,256,2048]{2,1,0:T(8,128)(2,1)}, u32[]{:S(2)}) copy-start(bf16[1,256,2048]{2,1,0:T(8,128)(2,1)} %param.11) | copy-start | bytes 3145732
  70.5 3.3 %copy-start.1 = (bf16[512,2048]{1,0:T(8,128)(2,1)S(1)}, bf16[512,2048]{1,0:T(8,128)(2,1)}, u32[]{:S(2)}) copy-start(bf16[512,2048]{1,0:T(8,128)(2,1)} %all-gather.7.cloned.1.call-done) | copy-start | bytes 6291460
  73.8 33.6 %copy-start.9 = (f32[8,1,64,256]{3,2,0,1:T(8,128)S(1)}, f32[8,1,64,256]{3,2,0,1:T(8,128)}, u32[]{:S(2)}) copy-start(f32[8,1,64,256]{3,2,0,1:T(8,128)} %convolution_bitcast_fusion.4) | copy-start | bytes 1572868
  74.5 36.1 %copy-start.11 = (f32[8,1,64,256]{3,2,0,1:T(8,128)}, f32[8,1,64,256]{3,2,0,1:T(8,128)S(1)}, u32[]{:S(2)}) copy-start(f32[8,1,64,256]{3,2,0,1:T(8,128)S(1)} %convolution_bitcast_fusion.3) | copy-start | bytes 1572868
  130.8 24.5 %all-to-all-start.3 = ((bf16[4,2,65536]{2,1,0:T(2,128)(2,1)}), bf16[4,2,65536]{2,1,0:T(2,128)(2,1)}, u32[]{:S(2)}, u32[]{:S(2)}) async-start(bf16[4,2,65536]{2,1,0:T(2,128)(2,1)} %reshape.242), calls=%async_computation.3 | async-start | bytes 2097152 | tf_op jit(solution)/shard_map/all_to_all | solution.py:79
  135.1 63.7 %all-gather.11.cloned.1.call-start = ((), (), s32[]{:S(2)}) async-start(), calls=%async_computation.10 | async-start | bytes 1310720 | tf_op jit(solution)/shard_map/all_gather | solution.py:76
  155.3 21.1 %all-to-all-start.4 = ((bf16[4,2,65536]{2,1,0:T(2,128)(2,1)}), bf16[4,2,65536]{2,1,0:T(2,128)(2,1)}, u32[]{:S(2)}, u32[]{:S(2)}) async-start(bf16[4,2,65536]{2,1,0:T(2,128)(2,1)} %reshape.244), calls=%async_computation.4 | async-start | bytes 2097152 | tf_op jit(solution)/shard_map/all_to_all | solution.py:80
  180.1 15.7 %copy-start.8 = (bf16[1,4,256,512]{3,2,1,0:T(8,128)(2,1)S(1)}, bf16[1,4,256,512]{3,2,1,0:T(8,128)(2,1)}, u32[]{:S(2)}) copy-start(bf16[1,4,256,512]{3,2,1,0:T(8,128)(2,1)} %copy.36) | copy-start | bytes 3145732
  191.3 10.6 %all-to-all-start.6 = ((f32[8,64,1]{1,2,0:T(1,128)}), f32[8,64,1]{1,2,0:T(1,128)S(1)}, u32[]{:S(2)}, u32[]{:S(2)}) async-start(f32[8,64,1]{1,2,0:T(1,128)} %psum.7), calls=%async_computation.6 | async-start | bytes 8192 | tf_op jit(solution)/shard_map/all_to_all | solution.py:89
  198.8 8.2 %copy-start.7 = (bf16[8,1,64,256]{3,2,0,1:T(8,128)(2,1)S(1)}, bf16[8,1,64,256]{3,2,0,1:T(8,128)(2,1)}, u32[]{:S(2)}) copy-start(bf16[8,1,64,256]{3,2,0,1:T(8,128)(2,1)} %get-tuple-element.21) | copy-start | bytes 786436
  201.9 20.4 %all-to-all-start.5 = ((bf16[8,64,512]{2,1,0:T(8,128)(2,1)}), bf16[8,64,512]{2,1,0:T(8,128)(2,1)S(1)}, u32[]{:S(2)}, u32[]{:S(2)}) async-start(bf16[8,64,512]{2,1,0:T(8,128)(2,1)} %fusion), calls=%async_computation.5 | async-start | bytes 1048576 | tf_op jit(solution)/shard_map/all_to_all | solution.py:86
  207.0 3.8 %copy-start.2 = (bf16[512,2048]{1,0:T(8,128)(2,1)S(1)}, bf16[512,2048]{1,0:T(8,128)(2,1)}, u32[]{:S(2)}) copy-start(bf16[512,2048]{1,0:T(8,128)(2,1)} %all-gather.7.cloned.1.call-done) | copy-start | bytes 6291460
  207.0 3.8 %copy-start.6 = (bf16[8,1,64,256]{3,2,0,1:T(8,128)(2,1)S(1)}, bf16[8,1,64,256]{3,2,0,1:T(8,128)(2,1)}, u32[]{:S(2)}) copy-start(bf16[8,1,64,256]{3,2,0,1:T(8,128)(2,1)} %get-tuple-element.22) | copy-start | bytes 786436
  210.8 2.1 copy-start.3
  210.8 2.1 copy-start.10
  210.8 2.3 copy-start.12
Sparse Core Ops, SparseCore 0:
  36.4 33.9 all-gather.6
  72.3 35.0 all-gather.4
  110.8 26.3 all-gather.8
  138.8 34.8 all-gather.10
where the time goes:
time: 233 us; the launch traced here: 231 us
  blocking collectives  57.7 us (25%)
  waiting for transfers between devices  48.6 us (21%)
  local copies, waits for them, and re-layouts  44.5 us (19%)
  other arithmetic  26.7 us (11%)
  matrix products  21.3 us (9%)
  starting transfers between devices  18.5 us (8%)
  between operations  14.1 us (6%)
    all_gather x1, waiting for transfers between devices, per_device(): lax.all_gather(part_cotangent, 'tp', axis=1, tiled=True)  32.8 us
    unnamed x40, local copies, waits for them, and re-layouts  26 us
    unnamed x2, other arithmetic  23.1 us
    all_to_all x1, blocking collectives, per_device(): lax.all_to_all(token_cols[token_of], 'ep', split_axis=0, concat_axis=0, t...  21.6 us
    all_to_all x1, blocking collectives, per_device(): lax.all_to_all(cotangent_cols[token_of], 'ep', split_axis=0, concat_axis=...  18.5 us
    all_to_all x1, waiting for transfers between devices, per_device(): lax.all_to_all(up_weight, 'tp', split_axis=2, concat_axis=1, tiled=True)  10.7 us
    psum x1, blocking collectives, per_device(): pair_products = lax.psum(jnp.sum(hidden * back_hidden, axis=3), 'tp')  9.53 us
    all_to_all x1, blocking collectives, per_device(): lax.all_to_all(send_weight, 'ep', split_axis=0, concat_axis=0, tiled=True)  8.07 us
  transfers between devices with their start and end apart: 8, of which 4 were waited for; matrix products, arithmetic and copies ran while one was open for 34% of the time, Pallas kernels for 0%

commit v1 on v0

--- a/solution.py
+++ b/solution.py
@@ -77,7 +77,12 @@
     )
     gate_cols, up_cols = (
         lax.all_to_all(gate_weight, "tp", split_axis=2, concat_axis=1, tiled=True),
-        lax.all_to_all(up_weight, "tp", split_axis=2, concat_axis=1, tiled=True),
+        jnp.concatenate(
+            lax.all_to_all(
+                jnp.stack(jnp.split(up_weight, lax.axis_size("tp"), axis=2)), "tp", 0, 0
+            ),
+            axis=1,
+        ),
     )
     pair_grad = (
         jnp.einsum("secf,efd->secd", full_gate, gate_cols, preferred_element_type=jnp.float32)

time: 233 us -> 216 us (0.927)
  local copies, waits for them, and re-layouts: 44.5 us -> 30.5 us
  other arithmetic: 26.7 us -> 16.2 us
  blocking collectives: 57.7 us -> 65.4 us
  waiting for transfers between devices: 48.6 us -> 52.4 us
  starting transfers between devices: 18.5 us -> 16 us
    all_to_all x1, waiting for transfers between devices: 0.01 us -> 12 us  [per_device(): lax.all_to_all(gate_weight, 'tp', split_axis=2, concat_axis=1, tiled=True)]
    unnamed x40 -> x38, local copies, waits for them, and re-layouts: 26 us -> 14.3 us
    unnamed x2 -> x1, other arithmetic: 23.1 us -> 11.6 us
    all_to_all x1, waiting for transfers between devices: 10.7 us -> 0.01 us  [per_device(): lax.all_to_all(jnp.stack(jnp.split(up_weight, lax.axis_size('tp'), axis=2...]
    psum x1, blocking collectives: 9.53 us -> 17.2 us  [per_device(): pair_products = lax.psum(jnp.sum(hidden * back_hidden, axis=3), 'tp')]
    all_to_all x1, waiting for transfers between devices: 0.01 us -> 2.37 us  [per_device(): lax.all_to_all(pair_products.reshape(buffer_rows), 'ep', split_axis=0, co...]
  transfers between devices with their start and end apart: 8 -> 8, of which waited for: 4 -> 5; matrix products, arithmetic and copies ran while one was open for 34% -> 25% of each run, Pallas kernels for 0% -> 0%
where the time goes in v1:
time: 216 us; the launch traced here: 215 us
  blocking collectives  65.4 us (30%)
  waiting for transfers between devices  52.4 us (24%)
  local copies, waits for them, and re-layouts  30.5 us (14%)
  matrix products  20.4 us (9%)
  other arithmetic  16.2 us (8%)
  starting transfers between devices  16 us (7%)
  between operations  14.1 us (7%)
    all_gather x1, waiting for transfers between devices, per_device(): lax.all_gather(part_cotangent, 'tp', axis=1, tiled=True)  32.8 us
    all_to_all x1, blocking collectives, per_device(): lax.all_to_all(token_cols[token_of], 'ep', split_axis=0, concat_axis=0, t...  21.6 us
    all_to_all x1, blocking collectives, per_device(): lax.all_to_all(cotangent_cols[token_of], 'ep', split_axis=0, concat_axis=...  18.5 us
    psum x1, blocking collectives, per_device(): pair_products = lax.psum(jnp.sum(hidden * back_hidden, axis=3), 'tp')  17.2 us
    unnamed x38, local copies, waits for them, and re-layouts  14.3 us
    all_to_all x1, waiting for transfers between devices, per_device(): lax.all_to_all(gate_weight, 'tp', split_axis=2, concat_axis=1, tiled=True)  12 us
    unnamed x1, other arithmetic  11.6 us
    all_to_all x1, blocking collectives, per_device(): lax.all_to_all(send_weight, 'ep', split_axis=0, concat_axis=0, tiled=True)  8.07 us
  transfers between devices with their start and end apart: 8, of which 5 were waited for; matrix products, arithmetic and copies ran while one was open for 25% of the time, Pallas kernels for 0%

profile of v1, /device:TPU:0, one launch (start us, length us, event | category | flops | bytes accessed | tf_op | source)
XLA Modules:
  0.0 214.9 jit_solution(410958308754793971)
XLA Ops:
  7.2 0.8 broadcast_multiply_fusion
  8.0 0.8 copy.27
  8.9 0.1 eq.25
  9.3 0.6 reduce-window.6
  9.9 0.2 slice_reduce_fusion
  10.3 1.4 scatter_custom_fusion
  11.7 1.0 constant_dynamic-slice_fusion
  12.7 2.0 gather_fusion.2
  14.7 21.6 %all_to_all.78 = bf16[8,64,512]{2,1,0:T(8,128)(2,1)} all-to-all(bf16[8,64,512]{2,1,0:T(8,128)(2,1)S(1)} %bitcast.120), channel_id=1, replica_groups=mesh['ep'=8,'tp'=4] {'ep'}, dimensions={0} | all-to-all | bytes 1048576 | tf_op jit(solution)/shard_map/all_to_all | solution.py:38
  36.4 2.0 gather_fusion.1
  38.4 18.5 %all_to_all.79 = bf16[8,64,512]{2,1,0:T(8,128)(2,1)} all-to-all(bf16[8,64,512]{2,1,0:T(8,128)(2,1)S(1)} %bitcast.119), channel_id=1, replica_groups=mesh['ep'=8,'tp'=4] {'ep'}, dimensions={0} | all-to-all | bytes 1048576 | tf_op jit(solution)/shard_map/all_to_all | solution.py:39
  57.1 0.1 reshape.158
  57.3 3.4 %gather_fusion = bf16[512]{0:T(512)(128)(2,1)S(1)} fusion(bf16[256]{0:T(256)(128)(2,1)S(1)} %reshape.158, s32[1024]{0:T(1024)S(1)} %get-tuple-element.32), kind=kCustom, calls=%fused_computation | custom fusion | bytes 4096 | tf_op jit(solution)/shard_map/gather | solution.py:33
  60.8 8.1 %all_to_all.80 = bf16[8,64,1]{1,2,0:T(2,128)(2,1)S(1)} all-to-all(bf16[8,64,1]{1,2,0:T(2,128)(2,1)S(1)} %all_to_all.70), channel_id=1, replica_groups=mesh['ep'=8,'tp'=4] {'ep'}, dimensions={0} | all-to-all | bytes 2048 | tf_op jit(solution)/shard_map/all_to_all | solution.py:40
  68.8 1.6 all-gather.7.cloned.1.call-done
  70.5 3.3 %convolution_bitcast_fusion.5 = f32[8,1,64,256]{3,2,0,1:T(8,128)} fusion(bf16[8,64,2048]{2,1,0:T(8,128)(2,1)} %bitcast.111, bf16[1,256,2048]{2,1,0:T(8,128)(2,1)S(1)} %copy-done.8), kind=kOutput, calls=%fused_computation.14 | convolution fusion | flops 536870912 | bytes 3670016 | tf_op jit(solution)/shard_map/secd,efd->secf/dot_general | solution.py:53
  73.7 0.7 convolution_bitcast_fusion.4
  74.5 32.8 %all-gather.5.cloned.1.call-done = bf16[512,2048]{1,0:T(8,128)(2,1)} async-done(((bf16[512,512]{1,0:T(8,128)(2,1)}), bf16[512,2048]{1,0:T(8,128)(2,1)}) %all-gather.5.cloned.1.call-update) | async-done | bytes 2097168 | tf_op jit(solution)/shard_map/all_gather | solution.py:44
  107.4 3.3 %multiply_reduce_fusion = (f32[8,64]{1,0:T(8,128)S(1)}, bf16[8,1,64,256]{3,2,0,1:T(8,128)(2,1)}, bf16[8,1,64,256]{3,2,0,1:T(8,128)(2,1)}) fusion(f32[8,1,64,256]{3,2,0,1:T(8,128)S(1)} %copy-done.10, f32[8,1,64,256]{3,2,0,1:T(8,128)S(1)} %convolution_bitcast_fusion.4, f32[8,64]{1,0:T(8,128)S(1)} %bitcast.124, bf16[8,64,2048]{2,1,0:T(8,128)(2,1)} %bitcast.117, ...), kind=kOutput, calls=%fused_computation.23 | convolution fusion | flops 539098624 | bytes 4722688 | tf_op jit(solution)/shard_map/secd,efd->secf/dot_general | solution.py:59
  110.7 4.6 %copy.31 = bf16[1,256,2048]{1,0,2:T(2,128)(2,1)S(1)} copy(bf16[1,256,2048]{2,1,0:T(8,128)(2,1)} %param.11) | data formatting | bytes 2097152 | tf_op args[4]
  115.3 0.5 broadcast.123
  115.8 11.6 %reduce.8 = bf16[2048,256]{1,0:T(8,128)(2,1)} reduce(bf16[2048,1,256]{2,1,0:T(2,128)(2,1)S(1)} %bitcast.115, bf16[]{:T(256)} %broadcast.123), dimensions={1}, to_apply=%bitcast.97.reduce_sub_computation | reduce | bytes 2097154
  127.4 3.6 %reshape.245 = bf16[4,2,65536]{2,1,0:T(2,128)(2,1)} reshape(bf16[2048,256]{1,0:T(8,128)(2,1)} %reduce.8) | data formatting | bytes 2097152
  130.9 3.5 %all-to-all-start.3 = ((bf16[4,2,65536]{2,1,0:T(2,128)(2,1)}), bf16[4,2,65536]{2,1,0:T(2,128)(2,1)S(1)}, u32[]{:S(2)}, u32[]{:S(2)}) async-start(bf16[4,2,65536]{2,1,0:T(2,128)(2,1)} %reshape.245), calls=%async_computation.3 | async-start | bytes 2097152 | tf_op jit(solution)/shard_map/all_to_all | solution.py:79
  134.5 0.5 all-gather.11.cloned.1.call-update
  135.2 1.1 pad_maximum_fusion
  136.3 12.0 %all-to-all-done.3 = bf16[4,2,65536]{2,1,0:T(2,128)(2,1)S(1)} async-done(((bf16[4,2,65536]{2,1,0:T(2,128)(2,1)}), bf16[4,2,65536]{2,1,0:T(2,128)(2,1)S(1)}, u32[]{:S(2)}, u32[]{:S(2)}) %all-to-all-start.3) | async-done | bytes 1048608 | tf_op jit(solution)/shard_map/all_to_all | solution.py:79
  148.2 4.2 %all-to-all-start.4 = ((bf16[4,1,256,512]{3,2,1,0:T(8,128)(2,1)}), bf16[4,1,256,512]{3,2,1,0:T(8,128)(2,1)}, u32[]{:S(2)}, u32[]{:S(2)}) async-start(bf16[4,1,256,512]{3,2,1,0:T(8,128)(2,1)} %pad_maximum_fusion), calls=%async_computation.4 | async-start | bytes 2097152 | tf_op jit(solution)/shard_map/all_to_all | solution.py:81
  152.5 2.6 %reshape.246 = bf16[2048,1,256]{2,1,0:T(2,128)(2,1)S(1)} reshape(bf16[4,2,65536]{2,1,0:T(2,128)(2,1)} %copy-done.3) | data formatting | bytes 2097152
  155.2 1.1 copy.34
  156.3 1.5 copy.32
  157.8 17.2 %psum.7 = f32[8,64,1]{1,2,0:T(1,128)} all-reduce(f32[8,64,1]{1,2,0:T(1,128)S(1)} %bitcast.128), channel_id=1, replica_groups=mesh['ep'=8,'tp'=4] {'tp'}, use_global_device_ids=true, to_apply=%region_6.7 | all-reduce | flops 512 | bytes 4096 | tf_op jit(solution)/shard_map/psum | solution.py:62
  175.0 1.9 convolution_bitcast_fusion.3
  176.9 4.6 %all-to-all-start.6 = ((f32[8,64,1]{1,2,0:T(1,128)}), f32[8,64,1]{1,2,0:T(1,128)S(1)}, u32[]{:S(2)}, u32[]{:S(2)}) async-start(f32[8,64,1]{1,2,0:T(1,128)} %psum.7), calls=%async_computation.6 | async-start | bytes 8192 | tf_op jit(solution)/shard_map/all_to_all | solution.py:94
  181.6 3.1 %fusion.1 = bf16[8,64,512]{2,1,0:T(8,128)(2,1)} fusion(f32[512,8,64]{0,2,1:T(8,128)S(1)} %convolution_bitcast_fusion.3, bf16[1024,512,1]{1,0,2:T(8,128)(2,1)} %bitcast.38, bf16[8,1,64,1024]{3,2,0,1:T(8,128)(2,1)} %all-gather.11.cloned.1.call-done), kind=kOutput, calls=%fused_computation.12 | convolution fusion | flops 537395200 | bytes 3670016 | tf_op jit(solution)/shard_map/secf,efd->secd/dot_general | solution.py:89
  184.7 2.4 %all-to-all-done.6 = f32[8,64,1]{1,2,0:T(1,128)S(1)} async-done(((f32[8,64,1]{1,2,0:T(1,128)}), f32[8,64,1]{1,2,0:T(1,128)S(1)}, u32[]{:S(2)}, u32[]{:S(2)}) %all-to-all-start.6) | async-done | bytes 2080 | tf_op jit(solution)/shard_map/all_to_all | solution.py:94
  187.0 3.5 %all-to-all-start.5 = ((bf16[8,64,512]{2,1,0:T(8,128)(2,1)}), bf16[8,64,512]{2,1,0:T(8,128)(2,1)S(1)}, u32[]{:S(2)}, u32[]{:S(2)}) async-start(bf16[8,64,512]{2,1,0:T(8,128)(2,1)} %fusion.1), calls=%async_computation.5 | async-start | bytes 1048576 | tf_op jit(solution)/shard_map/all_to_all | solution.py:91
  190.6 3.8 %convolution_bitcast_fusion.2 = f32[1,256,2048]{2,1,0:T(8,128)} fusion(bf16[8,64,2048]{2,1,0:T(8,128)(2,1)} %bitcast.112, bf16[8,1,64,256]{3,2,0,1:T(8,128)(2,1)S(1)} %copy-done.7), kind=kOutput, calls=%fused_computation.8 | convolution fusion | flops 536870912 | bytes 4456448 | tf_op jit(solution)/shard_map/secf,secd->efd/dot_general | solution.py:70
  194.4 2.0 convolution_bitcast_fusion.1
  196.4 0.2 copy-done.13
  196.7 2.2 %convolution_bitcast_fusion = f32[1,256,2048]{2,1,0:T(8,128)} fusion(bf16[8,64,2048]{2,1,0:T(8,128)(2,1)S(1)} %bitcast.118, f32[8,64]{1,0:T(8,128)S(1)} %bitcast.125, f32[8,1,64,256]{3,2,0,1:T(8,128)S(1)} %copy-done.11, f32[8,1,64,256]{3,2,0,1:T(8,128)S(1)} %copy-done.13), kind=kOutput, calls=%fused_computation.6 | convolution fusion | flops 537788416 | bytes 5244928 | tf_op jit(solution)/shard_map/secf,secd->efd/dot_general | solution.py:67
  198.8 0.5 broadcast.122
  199.3 0.7 reduce.7
  200.1 1.9 gather_fusion.4
  202.2 0.6 copy.33
  202.8 3.0 %all-to-all-done.5 = bf16[8,64,512]{2,1,0:T(8,128)(2,1)S(1)} async-done(((bf16[8,64,512]{2,1,0:T(8,128)(2,1)}), bf16[8,64,512]{2,1,0:T(8,128)(2,1)S(1)}, u32[]{:S(2)}, u32[]{:S(2)}) %all-to-all-start.5) | async-done | bytes 524320 | tf_op jit(solution)/shard_map/all_to_all | solution.py:91
  205.8 1.2 gather_fusion.3
  207.1 1.3 reduce_sum.36
  (59 shorter events, 1.5 us)
Async XLA Ops:
  7.2 100.2 %copy-start = (bf16[1,256,2048]{2,1,0:T(8,128)(2,1)S(1)}, bf16[1,256,2048]{2,1,0:T(8,128)(2,1)}, u32[]{:S(2)}) copy-start(bf16[1,256,2048]{2,1,0:T(8,128)(2,1)} %param.13) | copy-start | bytes 3145732
  7.2 63.3 %all-gather.7.cloned.1.call-start = ((), (), s32[]{:S(2)}) async-start(), calls=%async_computation.8 | async-start | bytes 2621440 | tf_op jit(solution)/shard_map/all_gather | solution.py:43
  36.3 71.0 %all-gather.5.cloned.1.call-start = ((), (), s32[]{:S(2)}) async-start(), calls=%async_computation.7 | async-start | bytes 2621440 | tf_op jit(solution)/shard_map/all_gather | solution.py:44
  36.4 20.6 %copy-start.14 = (bf16[128,2]{0,1:T(2,128)(2,1)S(1)}, bf16[128,2]{0,1:T(2,128)(2,1)}, u32[]{:S(2)}) copy-start(bf16[128,2]{0,1:T(2,128)(2,1)} %param.10) | copy-start | bytes 1540
  38.4 32.1 %copy-start.8 = (bf16[1,256,2048]{2,1,0:T(8,128)(2,1)S(1)}, bf16[1,256,2048]{2,1,0:T(8,128)(2,1)}, u32[]{:S(2)}) copy-start(bf16[1,256,2048]{2,1,0:T(8,128)(2,1)} %param.12) | copy-start | bytes 3145732
  56.9 118.0 %all-gather.9.cloned.1.call-start = ((), (), s32[]{:S(2)}) async-start(), calls=%async_computation.9 | async-start | bytes 1310720 | tf_op jit(solution)/shard_map/all_gather | solution.py:75
  60.6 13.1 %copy-start.5 = (bf16[1,256,2048]{2,1,0:T(8,128)(2,1)S(1)}, bf16[1,256,2048]{2,1,0:T(8,128)(2,1)}, u32[]{:S(2)}) copy-start(bf16[1,256,2048]{2,1,0:T(8,128)(2,1)} %param.11) | copy-start | bytes 3145732
  70.5 3.3 %copy-start.1 = (bf16[512,2048]{1,0:T(8,128)(2,1)S(1)}, bf16[512,2048]{1,0:T(8,128)(2,1)}, u32[]{:S(2)}) copy-start(bf16[512,2048]{1,0:T(8,128)(2,1)} %all-gather.7.cloned.1.call-done) | copy-start | bytes 6291460
  73.7 33.6 %copy-start.10 = (f32[8,1,64,256]{3,2,0,1:T(8,128)S(1)}, f32[8,1,64,256]{3,2,0,1:T(8,128)}, u32[]{:S(2)}) copy-start(f32[8,1,64,256]{3,2,0,1:T(8,128)} %convolution_bitcast_fusion.5) | copy-start | bytes 1572868
  74.5 36.2 %copy-start.12 = (f32[8,1,64,256]{3,2,0,1:T(8,128)}, f32[8,1,64,256]{3,2,0,1:T(8,128)S(1)}, u32[]{:S(2)}) copy-start(f32[8,1,64,256]{3,2,0,1:T(8,128)S(1)} %convolution_bitcast_fusion.4) | copy-start | bytes 1572868
  127.4 7.7 %copy-start.9 = (bf16[1,256,2048]{2,1,0:T(8,128)(2,1)S(1)}, bf16[1,256,2048]{2,1,0:T(8,128)(2,1)}, u32[]{:S(2)}) copy-start(bf16[1,256,2048]{2,1,0:T(8,128)(2,1)} %param.12) | copy-start | bytes 3145732
  130.9 17.3 %all-to-all-start.3 = ((bf16[4,2,65536]{2,1,0:T(2,128)(2,1)}), bf16[4,2,65536]{2,1,0:T(2,128)(2,1)S(1)}, u32[]{:S(2)}, u32[]{:S(2)}) async-start(bf16[4,2,65536]{2,1,0:T(2,128)(2,1)} %reshape.245), calls=%async_computation.3 | async-start | bytes 2097152 | tf_op jit(solution)/shard_map/all_to_all | solution.py:79
  134.5 47.1 %all-gather.11.cloned.1.call-start = ((), (), s32[]{:S(2)}) async-start(), calls=%async_computation.10 | async-start | bytes 1310720 | tf_op jit(solution)/shard_map/all_gather | solution.py:76
  148.2 4.3 %copy-start.3 = (bf16[4,2,65536]{2,1,0:T(2,128)(2,1)}, bf16[4,2,65536]{2,1,0:T(2,128)(2,1)S(1)}, u32[]{:S(2)}) copy-start(bf16[4,2,65536]{2,1,0:T(2,128)(2,1)S(1)} %all-to-all-done.3) | copy-start | bytes 3145732
  148.2 28.7 %all-to-all-start.4 = ((bf16[4,1,256,512]{3,2,1,0:T(8,128)(2,1)}), bf16[4,1,256,512]{3,2,1,0:T(8,128)(2,1)}, u32[]{:S(2)}, u32[]{:S(2)}) async-start(bf16[4,1,256,512]{3,2,1,0:T(8,128)(2,1)} %pad_maximum_fusion), calls=%async_computation.4 | async-start | bytes 2097152 | tf_op jit(solution)/shard_map/all_to_all | solution.py:81
  176.9 10.1 %all-to-all-start.6 = ((f32[8,64,1]{1,2,0:T(1,128)}), f32[8,64,1]{1,2,0:T(1,128)S(1)}, u32[]{:S(2)}, u32[]{:S(2)}) async-start(f32[8,64,1]{1,2,0:T(1,128)} %psum.7), calls=%async_computation.6 | async-start | bytes 8192 | tf_op jit(solution)/shard_map/all_to_all | solution.py:94
  181.6 9.0 %copy-start.7 = (bf16[8,1,64,256]{3,2,0,1:T(8,128)(2,1)S(1)}, bf16[8,1,64,256]{3,2,0,1:T(8,128)(2,1)}, u32[]{:S(2)}) copy-start(bf16[8,1,64,256]{3,2,0,1:T(8,128)(2,1)} %get-tuple-element.21) | copy-start | bytes 786436
  187.0 18.8 %all-to-all-start.5 = ((bf16[8,64,512]{2,1,0:T(8,128)(2,1)}), bf16[8,64,512]{2,1,0:T(8,128)(2,1)S(1)}, u32[]{:S(2)}, u32[]{:S(2)}) async-start(bf16[8,64,512]{2,1,0:T(8,128)(2,1)} %fusion.1), calls=%async_computation.5 | async-start | bytes 1048576 | tf_op jit(solution)/shard_map/all_to_all | solution.py:91
  190.6 3.8 %copy-start.2 = (bf16[512,2048]{1,0:T(8,128)(2,1)S(1)}, bf16[512,2048]{1,0:T(8,128)(2,1)}, u32[]{:S(2)}) copy-start(bf16[512,2048]{1,0:T(8,128)(2,1)} %all-gather.7.cloned.1.call-done) | copy-start | bytes 6291460
  190.6 3.8 %copy-start.6 = (bf16[8,1,64,256]{3,2,0,1:T(8,128)(2,1)S(1)}, bf16[8,1,64,256]{3,2,0,1:T(8,128)(2,1)}, u32[]{:S(2)}) copy-start(bf16[8,1,64,256]{3,2,0,1:T(8,128)(2,1)} %get-tuple-element.22) | copy-start | bytes 786436
  194.4 2.1 copy-start.4
  194.4 2.1 copy-start.11
  194.4 2.3 %copy-start.13 = (f32[8,1,64,256]{3,2,0,1:T(8,128)S(1)}, f32[8,1,64,256]{3,2,0,1:T(8,128)}, u32[]{:S(2)}) copy-start(f32[8,1,64,256]{3,2,0,1:T(8,128)} %copy-done.12) | copy-start | bytes 1572868
Sparse Core Ops, SparseCore 0:
  36.4 33.9 all-gather.6
  72.3 35.0 all-gather.4
  110.8 26.3 all-gather.8
  138.9 32.5 all-gather.10
